TPU v7x, 512 devices: a 8x2x16 block of a 8x8x16 slice. The times are simulated.
512 devices in a mesh: grp: 2 (over y), sp: 32 (over z, core), tp: 8 (over x).
Axes of the slice: x: 8, y: 2, z: 16, core: 2. Of those that a mesh axis runs over, the one named last changes fastest.
The devices are a block of a 8x8x16 slice.
Arguments:
- tokens: bfloat16 [32768, 2048], P(('grp', 'sp'), 'tp'), parts along dimension 0, may hold values from -140 to 140, as said below
- mix_gain: bfloat16 [2, 2048], replicated, may hold values from 0.099609375 to 1.8984375
- gate_weight: bfloat16 [2, 2048, 2048], P(None, 'sp', 'tp'), may hold values from -0.125 to 0.125
- mix_weight: bfloat16 [2, 2048, 2048], P(None, 'sp', 'tp'), may hold values from -0.125 to 0.125
- value_weight: bfloat16 [2, 2048, 2048], P(None, 'sp', 'tp'), may hold values from -0.125 to 0.125
- out_weight: bfloat16 [2, 2048, 2048], P(None, 'sp', 'tp'), may hold values from -0.125 to 0.125
- conv_taps: bfloat16 [2, 3, 2048], P(None, None, 'tp'), may hold values from -3.5 to 3.5
Outputs:
- result_stream: bfloat16 [32768, 2048], P(('grp', 'sp'), 'tp'), parts along dimension 0
There are 2 independent parts, one for each index of `grp`. A program takes and returns all parts, laid end to end along the dimension named above; an argument that names none is the same for every part. Nothing has to cross between parts.
Inputs may be any that keep to these rules, and one draw needn't show every extreme that they name: `tokens`: activations with feature scales of several sizes.
All inputs are finite; a program needn't handle non-finite values.
Results may differ from a plain program's by a relative error of at most 0.015.
Values may be sent and summed in bfloat16 or wider, within the bound.
No kernel may reach another device: no remote copies, remote signals or barrier semaphores. Data moves between devices by JAX's collectives and lax.ppermute only.
A program may use at most 64 MiB of HBM per device.

v0:
```python
import jax
import jax.numpy as jnp
from jax import lax
from jax.sharding import PartitionSpec as P

EPS = 1e-06


def passed_along(x, axis, by):
    devices = lax.axis_size(axis)
    pairs = [(i, i + by) for i in range(devices) if 0 <= i + by < devices]
    return lax.ppermute(x, axis, pairs)


def in_one_piece(arrays, axis, dim, along):
    ends, at = ([], 0)
    for a in arrays[:-1]:
        at += a.shape[along]
        ends.append(at)
    both = jnp.concatenate(arrays, axis=along)
    return tuple(jnp.split(lax.all_gather(both, axis, axis=dim, tiled=True), ends, axis=along))


def in_order(pieces, dim):
    dims = list(pieces.shape[1:])
    dims[dim] *= pieces.shape[0]
    return jnp.moveaxis(pieces, 0, dim).reshape(dims)


def copy_for_each(x, axis):
    copies = jnp.broadcast_to(x, (lax.axis_size(axis), *x.shape))
    return lax.all_to_all(copies, axis, split_axis=0, concat_axis=0, tiled=True)


def collect(x, axis, dim):
    return in_order(copy_for_each(x, axis), dim)


def normed_rows(rows, gain):
    wide_rows = rows.astype(jnp.float32)
    factor = lax.rsqrt(jnp.mean(wide_rows * wide_rows, axis=1, keepdims=True) + EPS)
    return (wide_rows * factor * gain.astype(jnp.float32)).astype(jnp.bfloat16)


def convolve(carried, before, tap_rows):
    padded = jnp.concatenate([before, carried], axis=0)
    row_count = carried.shape[0]
    result = jnp.zeros_like(carried)
    for tap_index in range(tap_rows.shape[0]):
        result = (
            result
            + tap_rows[tap_index].astype(jnp.float32) * padded[tap_index : tap_index + row_count]
        )
    return result


def shards(tokens, mix_gain, gate_weight, mix_weight, value_weight, out_weight, conv_taps):
    layer_count = gate_weight.shape[0]
    conv_reach = conv_taps.shape[1] - 1
    fringe_depth = conv_reach * layer_count
    before_rows = passed_along(tokens[tokens.shape[0] - fringe_depth :], "sp", 1)
    stream = jnp.concatenate([before_rows, tokens], axis=0)
    gathered = in_one_piece((gate_weight, mix_weight, value_weight, out_weight), "sp", 1, 0)
    channels = gate_weight.shape[2]
    for layer_index in range(layer_count):
        whole = collect(stream, "tp", 1)
        normed = normed_rows(whole, mix_gain[layer_index])
        gate = jnp.dot(normed, gathered[0][layer_index], preferred_element_type=jnp.float32)
        inner = jnp.dot(normed, gathered[1][layer_index], preferred_element_type=jnp.float32)
        values = jnp.dot(normed, gathered[2][layer_index], preferred_element_type=jnp.float32)
        gate = gate.astype(jnp.bfloat16)
        inner = inner.astype(jnp.bfloat16)
        values = values.astype(jnp.bfloat16)
        carried = inner.astype(jnp.float32) * values.astype(jnp.float32)
        before = jnp.zeros((conv_reach, channels), jnp.float32)
        conv = convolve(carried, before, conv_taps[layer_index])
        mixed = (gate.astype(jnp.float32) * conv).astype(jnp.bfloat16)
        mixed_all = lax.all_gather(mixed, "tp", axis=1, tiled=True)
        product = jnp.dot(mixed_all, gathered[3][layer_index], preferred_element_type=jnp.float32)
        stream = (stream.astype(jnp.float32) + product).astype(jnp.bfloat16)
    return stream[fringe_depth:]


def solution(mesh):
    return jax.shard_map(
        shards,
        mesh=mesh,
        in_specs=(
            P(("grp", "sp"), "tp"),
            P(),
            P(None, "sp", "tp"),
            P(None, "sp", "tp"),
            P(None, "sp", "tp"),
            P(None, "sp", "tp"),
            P(None, None, "tp"),
        ),
        out_specs=P(("grp", "sp"), "tp"),
        check_vma=False,
    )
```

profile of v0, /device:TPU:66, one launch (start us, length us, event | category | flops | bytes accessed | tf_op | source)
XLA Modules:
  0.0 306.0 jit_solution(15098368979078359198)
XLA Ops:
  6.6 1.7 pad_maximum_fusion.1
  8.3 0.7 slice.88
  9.0 1.8 collective-permute-start
  10.8 0.8 collective-permute-done
  11.6 1.0 pad_maximum_fusion
  12.6 1.5 broadcast_in_dim.4
  14.1 43.5 %all-to-all-start = ((bf16[8,516,256]{2,1,0:T(8,128)(2,1)}), bf16[8,516,256]{2,1,0:T(8,128)(2,1)S(1)}, u32[]{:S(2)}, u32[]{:S(2)}) async-start(bf16[8,516,256]{2,1,0:T(8,128)(2,1)} %broadcast_in_dim.4), calls=%async_computation | async-start | bytes 4259840 | tf_op jit(solution)/shard_map/all_to_all | solution.py:32
  57.8 51.2 %all-to-all-done = bf16[8,516,256]{2,1,0:T(8,128)(2,1)S(1)} async-done(((bf16[8,516,256]{2,1,0:T(8,128)(2,1)}), bf16[8,516,256]{2,1,0:T(8,128)(2,1)S(1)}, u32[]{:S(2)}, u32[]{:S(2)}) %all-to-all-start) | async-done | bytes 2113568 | tf_op jit(solution)/shard_map/all_to_all | solution.py:32
  109.0 0.5 fusion
  109.5 0.6 fusion.7
  110.0 0.4 copy.8
  110.5 0.1 pad.8
  110.6 0.7 copy.10
  111.3 12.6 %all-gather.4.cloned.1.call-done = bf16[8,2048,256]{2,1,0:T(8,128)(2,1)} async-done(((bf16[8,64,256]{2,1,0:T(8,128)(2,1)}), bf16[8,2048,256]{2,1,0:T(8,128)(2,1)}) %all-gather.4.cloned.1.call-update) | async-done | bytes 8388624 | tf_op jit(solution)/shard_map/all_gather | solution.py:21
  123.9 2.0 fusion.13
  125.9 2.0 fusion.12
  128.0 2.7 fusion.10
  130.8 49.9 %all-gather.6.cloned.1.call-done = bf16[516,2048]{1,0:T(8,128)(2,1)} async-done(((bf16[516,256]{1,0:T(8,128)(2,1)}), bf16[516,2048]{1,0:T(8,128)(2,1)}) %all-gather.6.cloned.1.call-update) | async-done | bytes 2113552 | tf_op jit(solution)/shard_map/all_gather | solution.py:78
  180.7 2.6 add_convert_fusion
  183.3 1.5 broadcast_in_dim.5
  184.8 5.6 %all-to-all-start.1 = ((bf16[8,516,256]{2,1,0:T(8,128)(2,1)}), bf16[8,516,256]{2,1,0:T(8,128)(2,1)S(1)}, u32[]{:S(2)}, u32[]{:S(2)}) async-start(bf16[8,516,256]{2,1,0:T(8,128)(2,1)} %broadcast_in_dim.5), calls=%async_computation.1 | async-start | bytes 4259840 | tf_op jit(solution)/shard_map/all_to_all | solution.py:32
  190.3 45.0 %all-to-all-done.1 = bf16[8,516,256]{2,1,0:T(8,128)(2,1)S(1)} async-done(((bf16[8,516,256]{2,1,0:T(8,128)(2,1)}), bf16[8,516,256]{2,1,0:T(8,128)(2,1)S(1)}, u32[]{:S(2)}, u32[]{:S(2)}) %all-to-all-start.1) | async-done | bytes 2113568 | tf_op jit(solution)/shard_map/all_to_all | solution.py:32
  235.3 0.5 fusion.3
  235.9 0.6 fusion.6
  236.4 0.4 copy.9
  237.0 0.7 copy.11
  237.7 2.0 fusion.19
  239.7 2.0 fusion.18
  241.7 2.7 fusion.16
  244.5 51.6 %all-gather.8.cloned.1.call-done = bf16[516,2048]{1,0:T(8,128)(2,1)} async-done(((bf16[516,256]{1,0:T(8,128)(2,1)}), bf16[516,2048]{1,0:T(8,128)(2,1)}) %all-gather.8.cloned.1.call-update) | async-done | bytes 2113552 | tf_op jit(solution)/shard_map/all_gather | solution.py:78
  296.0 2.6 fusion.20
  298.6 0.8 fusion.22
  (19 shorter events, 0.4 us)
Async XLA Ops:
  6.5 117.4 %all-gather.4.cloned.1.call-start = ((), (), s32[]{:S(2)}) async-start(), calls=%async_computation.2 | async-start | bytes 8650752 | tf_op jit(solution)/shard_map/all_gather | solution.py:21
  9.0 2.6 collective-permute-start
  14.1 43.5 %copy-start.1 = (bf16[2,2048]{1,0:T(2,128)(2,1)S(1)}, bf16[2,2048]{1,0:T(2,128)(2,1)}, u32[]{:S(2)}) copy-start(bf16[2,2048]{1,0:T(2,128)(2,1)} %param.8) | copy-start | bytes 24580
  14.1 43.6 %copy-start.2 = (bf16[2,3,256]{2,0,1:T(2,128)(2,1)S(1)}, bf16[2,3,256]{2,0,1:T(2,128)(2,1)}, u32[]{:S(2)}) copy-start(bf16[2,3,256]{2,0,1:T(2,128)(2,1)} %param.13) | copy-start | bytes 9220
  14.1 94.8 %all-to-all-start = ((bf16[8,516,256]{2,1,0:T(8,128)(2,1)}), bf16[8,516,256]{2,1,0:T(8,128)(2,1)S(1)}, u32[]{:S(2)}, u32[]{:S(2)}) async-start(bf16[8,516,256]{2,1,0:T(8,128)(2,1)} %broadcast_in_dim.4), calls=%async_computation | async-start | bytes 4259840 | tf_op jit(solution)/shard_map/all_to_all | solution.py:32
  57.7 123.0 %all-gather.6.cloned.1.call-start = ((), (), s32[]{:S(2)}) async-start(), calls=%async_computation.3 | async-start | bytes 2396160 | tf_op jit(solution)/shard_map/all_gather | solution.py:78
  127.9 52.7 %copy-start = (bf16[512,256]{1,0:T(8,128)(2,1)S(1)}, bf16[512,256]{1,0:T(8,128)(2,1)}, u32[]{:S(2)}) copy-start(bf16[512,256]{1,0:T(8,128)(2,1)} %param.7) | copy-start | bytes 786436
  184.8 50.6 %all-to-all-start.1 = ((bf16[8,516,256]{2,1,0:T(8,128)(2,1)}), bf16[8,516,256]{2,1,0:T(8,128)(2,1)S(1)}, u32[]{:S(2)}, u32[]{:S(2)}) async-start(bf16[8,516,256]{2,1,0:T(8,128)(2,1)} %broadcast_in_dim.5), calls=%async_computation.1 | async-start | bytes 4259840 | tf_op jit(solution)/shard_map/all_to_all | solution.py:32
  190.3 105.7 %all-gather.8.cloned.1.call-start = ((), (), s32[]{:S(2)}) async-start(), calls=%async_computation.4 | async-start | bytes 2396160 | tf_op jit(solution)/shard_map/all_gather | solution.py:78
Sparse Core Ops, SparseCore 0:
  9.5 114.3 all-gather.3
  130.9 49.7 all-gather.5
  244.6 51.3 all-gather.7
where the time goes:
time: 307 us; the launch traced here: 306 us
  waiting for transfers between devices  211 us (69%)
  starting transfers between devices  50.9 us (17%)
  matrix products  18.6 us (6%)
  between operations  13.3 us (4%)
  local copies, waits for them, and re-layouts  6.28 us (2%)
  other arithmetic  5.67 us (2%)
    all_gather x2, waiting for transfers between devices, shards(): mixed_all = lax.all_gather(mixed, 'tp', axis=1, tiled=True)  101 us
    all_to_all x2, waiting for transfers between devices, copy_for_each(): return lax.all_to_all(copies, axis, split_axis=0, concat_axis=0, tiled=True)  96.2 us
    all_to_all x2, starting transfers between devices, copy_for_each(): return lax.all_to_all(copies, axis, split_axis=0, concat_axis=0, tiled=True)  49.1 us
    all_gather x1, waiting for transfers between devices, in_one_piece(): lax.all_gather(both, axis, axis=dim, tiled=True)  12.6 us
  transfers between devices with their start and end apart: 6, of which 6 were waited for; matrix products, arithmetic and copies ran while one was open for 2% of the time, Pallas kernels for 0%

commit v1 on v0

--- a/solution.py
+++ b/solution.py
@@ -75,7 +75,9 @@
         before = jnp.zeros((conv_reach, channels), jnp.float32)
         conv = convolve(carried, before, conv_taps[layer_index])
         mixed = (gate.astype(jnp.float32) * conv).astype(jnp.bfloat16)
-        mixed_all = lax.all_gather(mixed, "tp", axis=1, tiled=True)
+        mixed_all = jnp.concatenate(
+            lax.all_to_all(jnp.stack([mixed] * lax.axis_size("tp")), "tp", 0, 0), axis=1
+        )
         product = jnp.dot(mixed_all, gathered[3][layer_index], preferred_element_type=jnp.float32)
         stream = (stream.astype(jnp.float32) + product).astype(jnp.bfloat16)
     return stream[fringe_depth:]

time: 307 us -> 322 us (1.049)
  the two profiles are of different devices: /device:TPU:66 before, /device:TPU:65 now
where the time goes in v1:
time: 322 us; the launch traced here: 321 us
  waiting for transfers between devices  152 us (47%)
  blocking collectives  112 us (35%)
  starting transfers between devices  15 us (5%)
  between operations  13.7 us (4%)
  local copies, waits for them, and re-layouts  11.1 us (3%)
  matrix products  11 us (3%)
  other arithmetic  5.67 us (2%)
    all_to_all x2, blocking collectives, shards(): lax.all_to_all(jnp.stack([mixed] * lax.axis_size('tp')), 'tp', 0, 0)  112 us
    all_to_all x2, waiting for transfers between devices, copy_for_each(): return lax.all_to_all(copies, axis, split_axis=0, concat_axis=0, tiled=True)  101 us
    ppermute x1, waiting for transfers between devices, passed_along(): return lax.ppermute(x, axis, pairs)  36.3 us
    all_gather x1, waiting for transfers between devices, in_one_piece(): lax.all_gather(both, axis, axis=dim, tiled=True)  15.4 us
    all_to_all x2, starting transfers between devices, copy_for_each(): return lax.all_to_all(copies, axis, split_axis=0, concat_axis=0, tiled=True)  7.93 us
    ppermute x1, starting transfers between devices, passed_along(): return lax.ppermute(x, axis, pairs)  7.05 us
  transfers between devices with their start and end apart: 4, of which 4 were waited for; matrix products, arithmetic and copies ran while one was open for 2% of the time, Pallas kernels for 0%

profile of v1, /device:TPU:65, one launch (start us, length us, event | category | flops | bytes accessed | tf_op | source)
XLA Modules:
  0.0 320.9 jit_solution(4269674332909985425)
XLA Ops:
  6.6 1.7 pad_maximum_fusion.1
  8.3 0.7 slice.88
  9.0 7.0 %collective-permute-start = (bf16[4,256]{1,0:T(4,128)(2,1)S(1)}, bf16[4,256]{1,0:T(4,128)(2,1)S(1)}, u32[]{:S(2)}, u32[]{:S(2)}) collective-permute-start(bf16[4,256]{1,0:T(4,128)(2,1)S(1)} %slice.88), channel_id=1, source_target_pairs={{0,8},{8,16},{16,24},{24,32},{32,40},{40,48},{48,56},{56,64},{64,7... | collective-permute-start | bytes 6152 | tf_op jit(solution)/shard_map/ppermute | solution.py:12
  16.0 36.3 %collective-permute-done = bf16[4,256]{1,0:T(4,128)(2,1)S(1)} collective-permute-done((bf16[4,256]{1,0:T(4,128)(2,1)S(1)}, bf16[4,256]{1,0:T(4,128)(2,1)S(1)}, u32[]{:S(2)}, u32[]{:S(2)}) %collective-permute-start) | collective-permute-done | bytes 2080 | tf_op jit(solution)/shard_map/ppermute | solution.py:12
  52.3 1.0 pad_maximum_fusion
  53.4 1.5 broadcast_in_dim.4
  54.9 3.9 %all-to-all-start = ((bf16[8,516,256]{2,1,0:T(8,128)(2,1)}), bf16[8,516,256]{2,1,0:T(8,128)(2,1)S(1)}, u32[]{:S(2)}, u32[]{:S(2)}) async-start(bf16[8,516,256]{2,1,0:T(8,128)(2,1)} %broadcast_in_dim.4), calls=%async_computation | async-start | bytes 4259840 | tf_op jit(solution)/shard_map/all_to_all | solution.py:32
  58.9 48.7 %all-to-all-done = bf16[8,516,256]{2,1,0:T(8,128)(2,1)S(1)} async-done(((bf16[8,516,256]{2,1,0:T(8,128)(2,1)}), bf16[8,516,256]{2,1,0:T(8,128)(2,1)S(1)}, u32[]{:S(2)}, u32[]{:S(2)}) %all-to-all-start) | async-done | bytes 2113568 | tf_op jit(solution)/shard_map/all_to_all | solution.py:32
  107.6 0.5 fusion
  108.1 0.6 fusion.7
  109.2 0.7 copy.12
  110.0 15.4 %all-gather.2.cloned.1.call-done = bf16[8,2048,256]{2,1,0:T(8,128)(2,1)} async-done(((bf16[8,64,256]{2,1,0:T(8,128)(2,1)}), bf16[8,2048,256]{2,1,0:T(8,128)(2,1)}) %all-gather.2.cloned.1.call-update) | async-done | bytes 8388624 | tf_op jit(solution)/shard_map/all_gather | solution.py:21
  125.3 2.0 fusion.13
  127.3 2.0 fusion.12
  129.3 2.0 fusion.10
  131.5 57.8 %all_to_all.20 = bf16[8,516,256]{2,1,0:T(8,128)(2,1)S(1)} all-to-all(bf16[8,516,256]{2,1,0:T(8,128)(2,1)S(1)} %stack.4), channel_id=1, replica_groups=mesh['grp'=2,'sp'=32,'tp'=8] {'tp'}, dimensions={0} | all-to-all | bytes 4227072 | tf_op jit(solution)/shard_map/all_to_all | solution.py:79
  189.8 0.7 copy.13
  190.7 2.0 add_convert_fusion
  192.7 1.5 broadcast_in_dim.5
  194.2 4.0 %all-to-all-start.2 = ((bf16[8,516,256]{2,1,0:T(8,128)(2,1)}), bf16[8,516,256]{2,1,0:T(8,128)(2,1)S(1)}, u32[]{:S(2)}, u32[]{:S(2)}) async-start(bf16[8,516,256]{2,1,0:T(8,128)(2,1)} %broadcast_in_dim.5), calls=%async_computation.2 | async-start | bytes 4259840 | tf_op jit(solution)/shard_map/all_to_all | solution.py:32
  198.2 52.1 %all-to-all-done.2 = bf16[8,516,256]{2,1,0:T(8,128)(2,1)S(1)} async-done(((bf16[8,516,256]{2,1,0:T(8,128)(2,1)}), bf16[8,516,256]{2,1,0:T(8,128)(2,1)S(1)}, u32[]{:S(2)}, u32[]{:S(2)}) %all-to-all-start.2) | async-done | bytes 2113568 | tf_op jit(solution)/shard_map/all_to_all | solution.py:32
  250.3 0.5 fusion.3
  250.8 0.5 fusion.6
  252.0 0.7 copy.14
  253.0 1.4 slice-done.1
  254.4 0.8 fusion.19
  255.2 0.8 fusion.18
  256.0 0.8 fusion.16
  256.9 54.2 %all_to_all.21 = bf16[8,516,256]{2,1,0:T(8,128)(2,1)S(1)} all-to-all(bf16[8,516,256]{2,1,0:T(8,128)(2,1)S(1)} %stack.5), channel_id=1, replica_groups=mesh['grp'=2,'sp'=32,'tp'=8] {'tp'}, dimensions={0} | all-to-all | bytes 4227072 | tf_op jit(solution)/shard_map/all_to_all | solution.py:79
  311.7 0.7 copy.15
  312.4 0.8 fusion.20
  313.2 0.8 fusion.22
  (28 shorter events, 3.2 us)
Async XLA Ops:
  6.5 118.8 %all-gather.2.cloned.1.call-start = ((), (), s32[]{:S(2)}) async-start(), calls=%async_computation.4 | async-start | bytes 8650752 | tf_op jit(solution)/shard_map/all_gather | solution.py:21
  9.0 43.4 %collective-permute-start = (bf16[4,256]{1,0:T(4,128)(2,1)S(1)}, bf16[4,256]{1,0:T(4,128)(2,1)S(1)}, u32[]{:S(2)}, u32[]{:S(2)}) collective-permute-start(bf16[4,256]{1,0:T(4,128)(2,1)S(1)} %slice.88), channel_id=1, source_target_pairs={{0,8},{8,16},{16,24},{24,32},{32,40},{40,48},{48,56},{56,64},{64,7... | collective-permute-start | bytes 6152 | tf_op jit(solution)/shard_map/ppermute | solution.py:12
  54.9 4.0 %copy-start.1 = (bf16[2,2048]{1,0:T(2,128)(2,1)S(1)}, bf16[2,2048]{1,0:T(2,128)(2,1)}, u32[]{:S(2)}) copy-start(bf16[2,2048]{1,0:T(2,128)(2,1)} %param.8) | copy-start | bytes 24580
  54.9 4.0 %copy-start.2 = (bf16[2,3,256]{2,0,1:T(2,128)(2,1)S(1)}, bf16[2,3,256]{2,0,1:T(2,128)(2,1)}, u32[]{:S(2)}) copy-start(bf16[2,3,256]{2,0,1:T(2,128)(2,1)} %param.13) | copy-start | bytes 9220
  54.9 52.7 %all-to-all-start = ((bf16[8,516,256]{2,1,0:T(8,128)(2,1)}), bf16[8,516,256]{2,1,0:T(8,128)(2,1)S(1)}, u32[]{:S(2)}, u32[]{:S(2)}) async-start(bf16[8,516,256]{2,1,0:T(8,128)(2,1)} %broadcast_in_dim.4), calls=%async_computation | async-start | bytes 4259840 | tf_op jit(solution)/shard_map/all_to_all | solution.py:32
  189.8 1.0 copy-start
  194.2 56.1 %all-to-all-start.2 = ((bf16[8,516,256]{2,1,0:T(8,128)(2,1)}), bf16[8,516,256]{2,1,0:T(8,128)(2,1)S(1)}, u32[]{:S(2)}, u32[]{:S(2)}) async-start(bf16[8,516,256]{2,1,0:T(8,128)(2,1)} %broadcast_in_dim.5), calls=%async_computation.2 | async-start | bytes 4259840 | tf_op jit(solution)/shard_map/all_to_all | solution.py:32
  250.8 2.2 slice-start
  251.4 3.0 slice-start.1
Sparse Core Ops, SparseCore 0:
  9.5 115.7 all-gather.1
